TPU v7x, 512 devices: a whole 4x4x16 slice. The times are simulated.
512 devices in a mesh: ep: 32 (over z, core), tp: 16 (over y, x).
Axes of the slice: x: 4, y: 4, z: 16, core: 2. Of those that a mesh axis runs over, the one named last changes fastest.
Arguments:
- mixer_rows: bfloat16 [8192, 2048], P('ep'), may hold values from -8 to 8
- mixer_gain: float32 [2048], replicated, may hold values from 0.1 to 1.9
- w_query: bfloat16 [2048, 1024], P(None, 'tp'), may hold values from -0.125 to 0.125
- w_key: bfloat16 [2048, 1024], P(None, 'tp'), may hold values from -0.125 to 0.125
- w_value: bfloat16 [2048, 1024], P(None, 'tp'), may hold values from -0.125 to 0.125
- key_shift: float32 [16, 8192], P('tp'), may hold values from -14 to 0
- w_out: bfloat16 [1024, 2048], P(None, 'tp'), may hold values from -0.75 to 0.75
- expert_rows: bfloat16 [4096, 2048], P('ep'), may hold values from -6 to 6
- expert_gain: float32 [2048], replicated, may hold values from 0.1 to 1.9
- routes: int32 [4096, 4], P('ep'), may hold values from 0 to 31, all different within a row; in each aligned block of 128 rows (0 to 127, 128 to 255, ...) at most 32 rows name the same one
- route_weight: float32 [4096, 4], P('ep'), may hold values from 0.05 to 0.6
- w_gate: bfloat16 [32, 2048, 2048], P('ep', None, 'tp'), may hold values from -0.25 to 0.25
- w_up: bfloat16 [32, 2048, 2048], P('ep', None, 'tp'), may hold values from -0.25 to 0.25
- w_down: bfloat16 [32, 2048, 2048], P('ep', None, 'tp'), may hold values from -0.0625 to 0.0625
Outputs:
- mixer_out: bfloat16 [8192, 2048], P('ep', 'tp')
- expert_out: bfloat16 [4096, 2048], P('ep', 'tp')
Inputs may be any that keep to these rules, and one draw needn't show every extreme that they name: `routes`: each row names 4 different experts. In each aligned block of 128 rows no expert is named by more than 32 rows, and in every draw some block names some expert exactly 32 times.
All inputs are finite; a program needn't handle non-finite values.
Results may differ from a plain program's by a relative error of at most 0.0073.
Values may be sent and summed in bfloat16 or wider, within the bound.
A program may use at most 64 MiB of HBM per device.

v0:
```python
import jax
import jax.numpy as jnp
from jax import lax
from jax.sharding import Mesh
from jax.sharding import PartitionSpec as P

EP = ("ep_0", "ep_1")
norm_eps = 1e-06
glu_limit = 7.0
glu_alpha = 1.702


def in_order(blocks, dim):
    shape = list(blocks.shape[1:])
    shape[dim] *= blocks.shape[0]
    return jnp.moveaxis(blocks, 0, dim).reshape(shape)


def all_blocks(shard, axes, turns):
    blocks = shard[None]
    for k in turns:
        blocks = lax.all_gather(blocks, axes[k], axis=0, tiled=True)
    carried = [lax.axis_size(axes[k]) for k in reversed(turns)]
    blocks = blocks.reshape(*carried, *shard.shape)
    turned = sorted(range(len(turns)), key=lambda place: turns[len(turns) - 1 - place])
    return blocks.transpose(*turned, *range(len(turns), blocks.ndim)).reshape(-1, *shard.shape)


def whole_of(shard, axes, turns, dim):
    return in_order(all_blocks(shard, axes, turns), dim)


def copy_for_each(shard, axis):
    devices = lax.axis_size(axis)
    return lax.all_to_all(
        jnp.broadcast_to(shard[None], (devices, *shard.shape)), axis, 0, 0, tiled=True
    )


def gather_directly(shard, axis, dim):
    blocks = copy_for_each(shard, axis)
    return in_order(blocks, dim)


def rms_scale(source, scaling):
    floats = source.astype(jnp.float32)
    inverse = lax.rsqrt(jnp.mean(floats * floats, axis=-1, keepdims=True) + norm_eps)
    return (floats * inverse * scaling).astype(jnp.bfloat16)


def stick_block(queries, packed, shifting, carried, allowed):
    length, head_count, head_width = queries.shape
    key_part = packed[:, : head_count * head_width].reshape(length, head_count, head_width)
    value_part = packed[:, head_count * head_width :].reshape(length, head_count, head_width)
    scores = jnp.einsum("thd,shd->hts", queries, key_part, preferred_element_type=jnp.float32)
    scores = scores * head_width ** (-0.5) + shifting[:, None, :]
    log_stay = jnp.where(allowed, jax.nn.log_sigmoid(-scores), 0.0)
    between = lax.cumsum(log_stay, axis=2, reverse=True) - log_stay
    weights = jnp.where(
        allowed, jnp.exp(jax.nn.log_sigmoid(scores) + between + carried[:, :, None]), 0.0
    )
    contrib = jnp.einsum(
        "hts,shd->thd", weights.astype(jnp.bfloat16), value_part, preferred_element_type=jnp.float32
    )
    return (contrib, carried + jnp.sum(log_stay, axis=2))


def per_device(
    mixer_rows,
    mixer_gain,
    w_query,
    w_key,
    w_value,
    key_shift,
    w_out,
    expert_rows,
    expert_gain,
    routes,
    route_weight,
    w_gate,
    w_up,
    w_down,
):
    length = mixer_rows.shape[0]
    head_count = key_shift.shape[0]
    head_width = w_query.shape[1] // head_count
    normed = rms_scale(mixer_rows, mixer_gain)
    queries = jnp.dot(normed, w_query, preferred_element_type=jnp.float32).astype(jnp.bfloat16)
    key_rows = jnp.dot(normed, w_key, preferred_element_type=jnp.float32).astype(jnp.bfloat16)
    value_rows = jnp.dot(normed, w_value, preferred_element_type=jnp.float32).astype(jnp.bfloat16)
    queries = queries.reshape(length, head_count, head_width)
    packed = jnp.concatenate([key_rows, value_rows], axis=1)
    device = lax.axis_index(EP)
    positions = jnp.arange(length, dtype=jnp.int32)
    strict = (positions[None, :] < positions[:, None])[None]
    own_shift = lax.dynamic_slice_in_dim(key_shift, device * length, length, 1)
    summed, carried = stick_block(
        queries, packed, own_shift, jnp.zeros((head_count, length), jnp.float32), strict
    )
    gathered = whole_of(packed, EP, (0, 1), 0)

    def visiting(offset, status):
        running, carry_now = status
        anchor = device - offset
        block_rows = lax.dynamic_slice_in_dim(gathered, anchor * length, length, 0)
        shifting = lax.dynamic_slice_in_dim(key_shift, anchor * length, length, 1)
        contrib, carry_now = stick_block(queries, block_rows, shifting, carry_now, True)
        return (running + contrib, carry_now)

    summed, carried = lax.fori_loop(1, device + 1, visiting, (summed, carried))
    head_out = summed.reshape(length, head_count * head_width).astype(jnp.bfloat16)
    weight_rows = w_out
    mixer_out = jnp.dot(
        gather_directly(head_out, "tp", 1), weight_rows, preferred_element_type=jnp.float32
    ).astype(jnp.bfloat16)
    tokens_here, top_count = routes.shape
    expert_count = lax.axis_size(EP)
    capacity = 2 * tokens_here * top_count // expert_count
    rows_after_norm = rms_scale(expert_rows, expert_gain)
    chosen = routes.reshape(-1)
    hit_table = (chosen[:, None] == jnp.arange(expert_count, dtype=jnp.int32)[None, :]).astype(
        jnp.int32
    )
    places = jnp.sum((jnp.cumsum(hit_table, axis=0) - 1) * hit_table, axis=1)
    targets = chosen * capacity + places
    assign_ids = jnp.arange(tokens_here * top_count, dtype=jnp.int32) // top_count
    owners = (
        jnp.full((expert_count * capacity,), tokens_here, jnp.int32).at[targets].set(assign_ids)
    )
    padded = jnp.concatenate(
        [rows_after_norm, jnp.zeros((1, rows_after_norm.shape[1]), jnp.bfloat16)], axis=0
    )
    outgoing = padded[owners].reshape(expert_count, capacity, rows_after_norm.shape[1])
    gate_cols = w_gate[0]
    upper_cols = w_up[0]
    down_rows = w_down[0]
    portion_size = capacity // lax.axis_size("tp")
    own_slots = lax.dynamic_slice_in_dim(
        outgoing, lax.axis_index("tp") * portion_size, portion_size, 1
    )
    arrived = lax.all_to_all(own_slots, EP, split_axis=0, concat_axis=0, tiled=True)
    expert_arrived = lax.all_gather(arrived, "tp", axis=1, tiled=True)
    expert_senders, slots_here, feature_count = expert_arrived.shape
    flat_rows = expert_arrived.reshape(expert_senders * slots_here, feature_count)
    gating = jnp.minimum(
        jnp.dot(flat_rows, gate_cols, preferred_element_type=jnp.float32), glu_limit
    )
    linear = jnp.clip(
        jnp.dot(flat_rows, upper_cols, preferred_element_type=jnp.float32), -glu_limit, glu_limit
    )
    hidden = gating * jax.nn.sigmoid(glu_alpha * gating) * (linear + 1.0)
    hidden = hidden.astype(jnp.bfloat16).reshape(expert_senders, slots_here, gate_cols.shape[1])
    senders = hidden.shape[0]
    slot_total = hidden.shape[1]
    portion_units = lax.all_gather(hidden, "tp", axis=2, tiled=True)
    weight_rows = down_rows
    flat_units = portion_units.reshape(senders * slot_total, portion_units.shape[2])
    results = jnp.dot(flat_units, weight_rows, preferred_element_type=jnp.float32)
    leaving = results.astype(jnp.bfloat16).reshape(senders, slot_total, down_rows.shape[1])
    returned = lax.all_to_all(leaving, EP, split_axis=0, concat_axis=0, tiled=True)
    picked = returned.reshape(expert_count * capacity, down_rows.shape[1])[targets].astype(
        jnp.float32
    )
    picked = picked * route_weight.reshape(-1)[:, None]
    expert_out = jnp.sum(picked.reshape(tokens_here, top_count, down_rows.shape[1]), axis=1).astype(
        jnp.bfloat16
    )
    return (mixer_out, expert_out)


def solution(mesh):
    torus = Mesh(mesh.devices.reshape(16, 2, mesh.shape["tp"]), ("ep_0", "ep_1", "tp"))
    return jax.shard_map(
        per_device,
        mesh=torus,
        in_specs=(
            P(EP, None),
            P(),
            P(None, "tp"),
            P(None, "tp"),
            P(None, "tp"),
            P("tp", None),
            P(None, "tp"),
            P(EP, None),
            P(),
            P(EP, None),
            P(EP, None),
            P(EP, None, "tp"),
            P(EP, None, "tp"),
            P(EP, None, "tp"),
        ),
        out_specs=(P(EP, "tp"), P(EP, "tp")),
        check_vma=False,
    )
```

profile of v0, /device:TPU:1, one launch (start us, length us, event | category | flops | bytes accessed | tf_op | source)
XLA Modules:
  0.0 366.4 jit_solution(1222065985565656454)
XLA Ops:
  7.3 1.6 fusion.17
  8.9 1.8 convolution_convert_fusion.2
  10.8 0.5 convolution_convert_fusion.4
  11.3 0.6 pad_maximum_fusion
  12.0 0.1 copy.63
  12.3 0.2 fusion.24
  12.5 1.2 reduce-window.26
  13.6 0.2 fusion.26
  13.9 0.2 slice_reduce_fusion
  14.1 0.1 eq.25
  14.2 0.1 copy.62
  14.3 0.1 mul.115
  14.6 2.4 scatter_custom_fusion
  17.1 6.0 %gather_fusion = bf16[1024,2048]{1,0:T(8,128)(2,1)} fusion(bf16[129,2048]{1,0:T(8,128)(2,1)S(1)} %concatenate.7, s32[1024]{0:T(1024)S(1)} %fusion.44), kind=kCustom, calls=%fused_computation | custom fusion | bytes 8392704 | tf_op jit(solution)/shard_map/gather | solution.py:133
  23.1 1.5 constant_dynamic-slice_fusion.1
  24.6 40.3 %all_to_all.15 = bf16[32,2,2048]{2,1,0:T(2,128)(2,1)S(1)} all-to-all(bf16[32,2,2048]{2,1,0:T(2,128)(2,1)S(1)} %constant_dynamic-slice_fusion.1), channel_id=1, replica_groups=mesh['ep_0'=16,'ep_1'=2,'tp'=16] {'ep_0','ep_1'}, dimensions={0} | all-to-all | bytes 524288 | tf_op jit(solution)/shard_map/all_to_all | solution.py:141
  64.9 0.8 copy.66
  65.8 19.3 %all-gather.12.cloned.1.call-done = bf16[4096,128]{0,1:T(8,128)(2,1)} async-done(((bf16[256,128]{0,1:T(8,128)(2,1)}), bf16[4096,128]{0,1:T(8,128)(2,1)}) %all-gather.12.cloned.1.call-update) | async-done | bytes 1048592 | tf_op jit(solution)/shard_map/all_gather | solution.py:22
  85.1 2.5 copy.70
  87.6 0.2 all-gather.10.cloned.1.call-start
  87.8 72.1 %all-gather.8.cloned.1.call-done = bf16[32,32,2048]{2,0,1:T(8,128)(2,1)} async-done(((bf16[32,2,2048]{2,0,1:T(8,128)(2,1)}), bf16[32,32,2048]{2,0,1:T(8,128)(2,1)}) %all-gather.8.cloned.1.call-update) | async-done | bytes 4194320 | tf_op jit(solution)/shard_map/all_gather | solution.py:142
  159.9 4.5 %copy.67 = bf16[32,32,2048]{2,1,0:T(8,128)(2,1)S(1)} copy(bf16[32,32,2048]{2,0,1:T(8,128)(2,1)} %all-gather.8.cloned.1.call-done) | data formatting | bytes 8388608 | tf_op jit(solution)/shard_map/all_gather | solution.py:142
  164.4 1.3 convolution_minimum_fusion
  165.7 2.0 fusion.22
  167.7 0.7 constant_dynamic-slice_fusion.2
  168.4 0.5 convolution_convert_fusion.3
  168.9 0.4 fusion.50
  169.3 2.3 fusion.39
  171.6 0.3 fusion.34
  171.9 0.1 convolution_bitcast_fusion.1
  172.1 12.4 %all-gather.6.cloned.1.call-done = bf16[32,256,128]{1,0,2:T(8,128)(2,1)} async-done(((bf16[16,256,128]{1,0,2:T(8,128)(2,1)}), bf16[32,256,128]{1,0,2:T(8,128)(2,1)}) %all-gather.6.cloned.1.call-update) | async-done | bytes 2097168 | tf_op jit(solution)/shard_map/all_gather | solution.py:22
  184.5 3.5 copy.61
  187.9 4.1 %while.12 = (s32[]{:T(128)}, f32[256,1,64]{0,2,1:T(8,128)S(1)}, f32[1,256]{1,0:T(1,128)S(1)}, s32[]{:T(128)}, s32[]{:T(128)}, /*index=5*/bf16[8192,128]{1,0:T(8,...) while((s32[]{:T(128)}, f32[256,1,64]{0,2,1:T(8,128)S(1)}, ...), condition=%wide.region_8.9_spmd, body=%wide.region_4.8_spmd.sunk | while | flops 27083784 | bytes 2680031 | solution.py:110
  188.0 0.7 constant_dynamic-slice_fusion.4
  188.7 0.3 fusion.77
  189.0 2.3 fusion.78
  191.4 0.4 fusion.79
  191.7 0.3 fusion.80
  192.1 0.8 broadcast_in_dim.17
  192.9 5.5 %all-to-all-start = ((bf16[16,256,64]{1,2,0:T(8,128)(2,1)}), bf16[16,256,64]{1,2,0:T(8,128)(2,1)S(1)}, u32[]{:S(2)}, u32[]{:S(2)}) async-start(bf16[16,256,64]{1,2,0:T(8,128)(2,1)} %broadcast_in_dim.17), calls=%async_computation | async-start | bytes 1048576 | tf_op jit(solution)/shard_map/all_to_all | solution.py:35
  198.4 59.6 %all-gather.10.cloned.1.call-done = bf16[32,32,2048]{2,1,0:T(8,128)(2,1)} async-done(((bf16[32,32,128]{2,1,0:T(8,128)(2,1)}), bf16[32,32,2048]{2,1,0:T(8,128)(2,1)}) %all-gather.10.cloned.1.call-update) | async-done | bytes 4194320 | tf_op jit(solution)/shard_map/all_gather | solution.py:155
  258.0 4.3 %convolution_convert_fusion = bf16[1024,128]{1,0:T(8,128)(2,1)} fusion(bf16[1024,2048]{1,0:T(8,128)(2,1)} %bitcast.152, bf16[1,2048,128]{2,1,0:T(8,128)(2,1)} %param.29), kind=kOutput, calls=%fused_computation.40 | convolution fusion | flops 537001984 | bytes 4980736 | tf_op jit(solution)/shard_map/dot_general | solution.py:158
  262.3 73.1 %all-to-all-start.2 = ((bf16[32,32,128]{2,1,0:T(8,128)(2,1)}), bf16[32,32,128]{2,1,0:T(8,128)(2,1)S(1)}, u32[]{:S(2)}, u32[]{:S(2)}) async-start(bf16[32,32,128]{2,1,0:T(8,128)(2,1)} %bitcast.38), calls=%async_computation.2 | async-start | bytes 524288 | tf_op jit(solution)/shard_map/all_to_all | solution.py:160
  335.4 0.1 copy.68
  335.5 1.0 convolution_convert_fusion.1
  336.5 21.1 %all-to-all-done.2 = bf16[32,32,128]{2,1,0:T(8,128)(2,1)S(1)} async-done(((bf16[32,32,128]{2,1,0:T(8,128)(2,1)}), bf16[32,32,128]{2,1,0:T(8,128)(2,1)S(1)}, u32[]{:S(2)}, u32[]{:S(2)}) %all-to-all-start.2) | async-done | bytes 262176 | tf_op jit(solution)/shard_map/all_to_all | solution.py:160
  357.6 1.3 gather_fusion.1
  359.0 0.9 fusion.37
  (54 shorter events, 0.7 us)
Async XLA Ops:
  7.2 157.2 %copy-start = (bf16[1,2048,128]{2,1,0:T(8,128)(2,1)S(1)}, bf16[1,2048,128]{2,1,0:T(8,128)(2,1)}, u32[]{:S(2)}) copy-start(bf16[1,2048,128]{2,1,0:T(8,128)(2,1)} %param.27) | copy-start | bytes 1572868
  7.2 3.6 copy-start.2
  7.2 3.6 copy-start.10
  7.2 3.6 copy-start.8
  7.2 77.9 %all-gather.12.cloned.1.call-start = ((), (), s32[]{:S(2)}) async-start(), calls=%async_computation.6 | async-start | bytes 1114112 | tf_op jit(solution)/shard_map/all_gather | solution.py:22
  8.9 3.1 copy-start.5
  8.9 3.4 copy-start.1
  10.8 2.9 copy-start.4
  12.0 147.9 %all-gather.8.cloned.1.call-start = ((), (), s32[]{:S(2)}) async-start(), calls=%async_computation.4 | async-start | bytes 4456448 | tf_op jit(solution)/shard_map/all_gather | solution.py:142
  65.8 118.7 %all-gather.6.cloned.1.call-start = ((), (), s32[]{:S(2)}) async-start(), calls=%async_computation.3 | async-start | bytes 3145728 | tf_op jit(solution)/shard_map/all_gather | solution.py:22
  87.6 170.4 %all-gather.10.cloned.1.call-start = ((), (), s32[]{:S(2)}) async-start(), calls=%async_computation.5 | async-start | bytes 4456448 | tf_op jit(solution)/shard_map/all_gather | solution.py:155
  164.4 1.3 copy-start.7
  165.7 2.7 copy-start.9
  192.9 69.4 %all-to-all-start = ((bf16[16,256,64]{1,2,0:T(8,128)(2,1)}), bf16[16,256,64]{1,2,0:T(8,128)(2,1)S(1)}, u32[]{:S(2)}, u32[]{:S(2)}) async-start(bf16[16,256,64]{1,2,0:T(8,128)(2,1)} %broadcast_in_dim.17), calls=%async_computation | async-start | bytes 1048576 | tf_op jit(solution)/shard_map/all_to_all | solution.py:35
  258.0 77.4 %copy-start.6 = (f32[128,4]{0,1:T(4,128)S(1)}, f32[128,4]{0,1:T(4,128)}, u32[]{:S(2)}) copy-start(f32[128,4]{0,1:T(4,128)} %param.26) | copy-start | bytes 6148
  258.0 77.5 %copy-start.3 = (bf16[1024,128]{1,0:T(8,128)(2,1)S(1)}, bf16[1024,128]{1,0:T(8,128)(2,1)}, u32[]{:S(2)}) copy-start(bf16[1024,128]{1,0:T(8,128)(2,1)} %param.22) | copy-start | bytes 786436
  262.3 95.3 %all-to-all-start.2 = ((bf16[32,32,128]{2,1,0:T(8,128)(2,1)}), bf16[32,32,128]{2,1,0:T(8,128)(2,1)S(1)}, u32[]{:S(2)}, u32[]{:S(2)}) async-start(bf16[32,32,128]{2,1,0:T(8,128)(2,1)} %bitcast.38), calls=%async_computation.2 | async-start | bytes 524288 | tf_op jit(solution)/shard_map/all_to_all | solution.py:160
Sparse Core Ops, SparseCore 0:
  12.1 72.9 all-gather.11
  88.1 71.7 all-gather.7
  162.0 22.4 all-gather.5
  187.3 70.6 all-gather.9
where the time goes:
time: 367 us; the launch traced here: 366 us
  waiting for transfers between devices  185 us (50%)
  starting transfers between devices  79 us (22%)
  blocking collectives  40.3 us (11%)
  local copies, waits for them, and re-layouts  25.8 us (7%)
  between operations  14.1 us (4%)
  matrix products  12.4 us (3%)
  other arithmetic  10.2 us (3%)
    all_to_all x1, starting transfers between devices, per_device(): lax.all_to_all(leaving, EP, split_axis=0, concat_axis=0, tiled=True)  73.1 us
    all_gather x1, waiting for transfers between devices, per_device(): expert_arrived = lax.all_gather(arrived, 'tp', axis=1, tiled=True)  72.1 us
    all_gather x1, waiting for transfers between devices, per_device(): portion_units = lax.all_gather(hidden, 'tp', axis=2, tiled=True)  59.6 us
    all_to_all x1, blocking collectives, per_device(): lax.all_to_all(own_slots, EP, split_axis=0, concat_axis=0, tiled=True)  40.3 us
    all_gather x2, waiting for transfers between devices, all_blocks(): blocks = lax.all_gather(blocks, axes[k], axis=0, tiled=True)  31.7 us
    all_to_all x1, waiting for transfers between devices, per_device(): lax.all_to_all(leaving, EP, split_axis=0, concat_axis=0, tiled=True)  21.1 us
  transfers between devices with their start and end apart: 6, of which 5 were waited for; matrix products, arithmetic and copies ran while one was open for 11% of the time, Pallas kernels for 0%

commit v1 on v0

--- a/solution.py
+++ b/solution.py
@@ -139,7 +139,14 @@
         outgoing, lax.axis_index("tp") * portion_size, portion_size, 1
     )
     arrived = lax.all_to_all(own_slots, EP, split_axis=0, concat_axis=0, tiled=True)
-    expert_arrived = lax.all_gather(arrived, "tp", axis=1, tiled=True)
+    n = lax.psum(1, "tp")
+    expert_arrived = lax.all_to_all(
+        jnp.tile(arrived, tuple((n if w == 1 else 1 for w in range(arrived.ndim)))),
+        "tp",
+        split_axis=1,
+        concat_axis=1,
+        tiled=True,
+    )
     expert_senders, slots_here, feature_count = expert_arrived.shape
     flat_rows = expert_arrived.reshape(expert_senders * slots_here, feature_count)
     gating = jnp.minimum(

time: 367 us -> 344 us (0.937)
  blocking collectives: 40.3 us -> 0 us
  starting transfers between devices: 79 us -> 103 us
  waiting for transfers between devices: 185 us -> 174 us
    all_gather x1 -> x0, waiting for transfers between devices: 72.1 us -> none  [per_device(): expert_arrived = lax.all_gather(arrived, 'tp', axis=1, tiled=True)]
    all_to_all x1 -> x0, blocking collectives: 40.3 us -> none  [per_device(): lax.all_to_all(own_slots, EP, split_axis=0, concat_axis=0, tiled=True)]
    all_gather x2, waiting for transfers between devices: 31.7 us -> 69.4 us  [all_blocks(): blocks = lax.all_gather(blocks, axes[k], axis=0, tiled=True)]
    all_to_all x0 -> x2, starting transfers between devices: none -> 23.7 us  [the longest x1 16.7 us: per_device(): lax.all_to_all(own_slots, EP, split_axis=0, concat_axis=0, tiled=True)]
    all_to_all x0 -> x2, waiting for transfers between devices: none -> 23.6 us  [the longest x1 22 us: per_device(): lax.all_to_all(own_slots, EP, split_axis=0, concat_axis=0, tiled=True)]
    all_to_all x0 -> x1, local copies, waits for them, and re-layouts: none -> 4.49 us  [per_device(): lax.all_to_all(jnp.tile(arrived, tuple((n if w == 1 else 1 for w in range...]
    all_gather x1 -> x0, local copies, waits for them, and re-layouts: 4.49 us -> none  [per_device(): expert_arrived = lax.all_gather(arrived, 'tp', axis=1, tiled=True)]
  transfers between devices with their start and end apart: 6 -> 7, of which waited for: 5 -> 6; matrix products, arithmetic and copies ran while one was open for 11% -> 9% of each run, Pallas kernels for 0% -> 0%
where the time goes in v1:
time: 344 us; the launch traced here: 343 us
  waiting for transfers between devices  174 us (51%)
  starting transfers between devices  103 us (30%)
  local copies, waits for them, and re-layouts  29.4 us (9%)
  between operations  14 us (4%)
  other arithmetic  11.6 us (3%)
  matrix products  11.1 us (3%)
    all_to_all x1, starting transfers between devices, per_device(): lax.all_to_all(leaving, EP, split_axis=0, concat_axis=0, tiled=True)  73 us
    all_gather x2, waiting for transfers between devices, all_blocks(): blocks = lax.all_gather(blocks, axes[k], axis=0, tiled=True)  69.4 us
    all_gather x1, waiting for transfers between devices, per_device(): portion_units = lax.all_gather(hidden, 'tp', axis=2, tiled=True)  59.6 us
    all_to_all x1, waiting for transfers between devices, per_device(): lax.all_to_all(own_slots, EP, split_axis=0, concat_axis=0, tiled=True)  22 us
    all_to_all x1, waiting for transfers between devices, per_device(): lax.all_to_all(leaving, EP, split_axis=0, concat_axis=0, tiled=True)  21.1 us
    all_to_all x1, starting transfers between devices, per_device(): lax.all_to_all(own_slots, EP, split_axis=0, concat_axis=0, tiled=True)  16.7 us
    all_to_all x1, starting transfers between devices, per_device(): lax.all_to_all(jnp.tile(arrived, tuple((n if w == 1 else 1 for w in range...  6.94 us
  transfers between devices with their start and end apart: 7, of which 6 were waited for; matrix products, arithmetic and copies ran while one was open for 9% of the time, Pallas kernels for 0%

profile of v1, /device:TPU:1, one launch (start us, length us, event | category | flops | bytes accessed | tf_op | source)
XLA Modules:
  0.0 342.6 jit_solution(11334325279424873342)
XLA Ops:
  7.2 0.8 copy.51
  8.2 0.7 broadcast_multiply_fusion
  8.9 1.2 reduce-window.26
  10.1 0.2 slice_reduce_fusion
  10.7 2.4 scatter_custom_fusion
  13.2 1.2 fusion.24
  14.4 1.2 fusion.26
  15.7 6.0 %gather_fusion = bf16[1024,2048]{1,0:T(8,128)(2,1)} fusion(bf16[129,2048]{1,0:T(8,128)(2,1)S(1)} %concatenate.7, s32[1024]{0:T(1024)S(1)} %fusion.44), kind=kCustom, calls=%fused_computation | custom fusion | bytes 8392704 | tf_op jit(solution)/shard_map/gather | solution.py:133
  21.8 2.2 constant_dynamic-slice_fusion.1
  23.9 16.7 %all-to-all-start.1 = ((bf16[32,2,2048]{2,1,0:T(2,128)(2,1)}), bf16[32,2,2048]{2,1,0:T(2,128)(2,1)S(1)}, u32[]{:S(2)}, u32[]{:S(2)}) async-start(bf16[32,2,2048]{2,1,0:T(2,128)(2,1)} %constant_dynamic-slice_fusion.1), calls=%async_computation.1 | async-start | bytes 524288 | tf_op jit(solution)/shard_map/all_to_all | solution.py:141
  40.7 0.3 fusion.17
  41.0 22.0 %all-to-all-done.1 = bf16[32,2,2048]{2,1,0:T(2,128)(2,1)S(1)} async-done(((bf16[32,2,2048]{2,1,0:T(2,128)(2,1)}), bf16[32,2,2048]{2,1,0:T(2,128)(2,1)S(1)}, u32[]{:S(2)}, u32[]{:S(2)}) %all-to-all-start.1) | async-done | bytes 262176 | tf_op jit(solution)/shard_map/all_to_all | solution.py:141
  63.0 2.5 tile.4
  65.5 6.9 %all-to-all-start.2 = ((bf16[32,32,2048]{2,0,1:T(8,128)(2,1)}), bf16[32,32,2048]{2,0,1:T(8,128)(2,1)}, u32[]{:S(2)}, u32[]{:S(2)}) async-start(bf16[32,32,2048]{2,0,1:T(8,128)(2,1)} %bitcast.132), calls=%async_computation.2 | async-start | bytes 8388608 | tf_op jit(solution)/shard_map/all_to_all | solution.py:143
  72.6 0.5 convolution_convert_fusion.2
  73.1 0.3 copy-done.6
  73.4 0.5 convolution_convert_fusion.4
  73.9 0.6 pad_maximum_fusion
  74.7 55.9 %all-gather.9.cloned.1.call-done = bf16[4096,128]{0,1:T(8,128)(2,1)} async-done(((bf16[256,128]{0,1:T(8,128)(2,1)}), bf16[4096,128]{0,1:T(8,128)(2,1)}) %all-gather.9.cloned.1.call-update) | async-done | bytes 1048592 | tf_op jit(solution)/shard_map/all_gather | solution.py:22
  130.6 2.5 copy.58
  133.1 0.2 all-gather.7.cloned.1.call-start
  133.3 1.7 all-to-all-done.2
  135.0 4.5 %copy.55 = bf16[32,32,2048]{2,1,0:T(8,128)(2,1)S(1)} copy(bf16[32,32,2048]{2,0,1:T(8,128)(2,1)} %all-to-all-done.2) | data formatting | bytes 8388608 | tf_op jit(solution)/shard_map/all_to_all | solution.py:143
  139.5 1.3 convolution_minimum_fusion
  140.8 2.0 fusion.22
  142.8 0.7 constant_dynamic-slice_fusion.2
  143.4 0.5 convolution_convert_fusion.3
  144.0 0.4 fusion.50
  144.3 2.3 fusion.39
  146.7 0.3 fusion.34
  147.0 0.1 convolution_bitcast_fusion.1
  147.2 13.5 %all-gather.5.cloned.1.call-done = bf16[32,256,128]{1,0,2:T(8,128)(2,1)} async-done(((bf16[16,256,128]{1,0,2:T(8,128)(2,1)}), bf16[32,256,128]{1,0,2:T(8,128)(2,1)}) %all-gather.5.cloned.1.call-update) | async-done | bytes 2097168 | tf_op jit(solution)/shard_map/all_gather | solution.py:22
  160.6 3.6 %copy.49 = bf16[2,16,256,128]{3,2,0,1:T(8,128)(2,1)S(1)} copy(bf16[2,16,256,128]{2,1,0,3:T(8,128)(2,1)} %bitcast.140) | data formatting | bytes 4194304 | tf_op jit(solution)/shard_map/reshape | solution.py:24
  164.2 4.1 %while.12 = (s32[]{:T(128)}, f32[256,1,64]{0,2,1:T(8,128)S(1)}, f32[1,256]{1,0:T(1,128)S(1)}, s32[]{:T(128)}, s32[]{:T(128)}, /*index=5*/bf16[8192,128]{1,0:T(8,...) while((s32[]{:T(128)}, f32[256,1,64]{0,2,1:T(8,128)S(1)}, ...), condition=%wide.region_8.9_spmd, body=%wide.region_4.8_spmd.sunk | while | flops 27083784 | bytes 2680031 | solution.py:110
  164.2 0.7 constant_dynamic-slice_fusion.4
  164.9 0.3 fusion.77
  165.2 2.3 fusion.78
  167.6 0.4 fusion.79
  168.0 0.3 fusion.80
  168.3 0.8 broadcast_in_dim.17
  169.2 5.5 %all-to-all-start = ((bf16[16,256,64]{1,2,0:T(8,128)(2,1)}), bf16[16,256,64]{1,2,0:T(8,128)(2,1)S(1)}, u32[]{:S(2)}, u32[]{:S(2)}) async-start(bf16[16,256,64]{1,2,0:T(8,128)(2,1)} %broadcast_in_dim.17), calls=%async_computation | async-start | bytes 1048576 | tf_op jit(solution)/shard_map/all_to_all | solution.py:35
  174.7 59.6 %all-gather.7.cloned.1.call-done = bf16[32,32,2048]{2,1,0:T(8,128)(2,1)} async-done(((bf16[32,32,128]{2,1,0:T(8,128)(2,1)}), bf16[32,32,2048]{2,1,0:T(8,128)(2,1)}) %all-gather.7.cloned.1.call-update) | async-done | bytes 4194320 | tf_op jit(solution)/shard_map/all_gather | solution.py:162
  234.3 4.3 %convolution_convert_fusion = bf16[1024,128]{1,0:T(8,128)(2,1)} fusion(bf16[1024,2048]{1,0:T(8,128)(2,1)} %bitcast.154, bf16[1,2048,128]{2,1,0:T(8,128)(2,1)} %param.29), kind=kOutput, calls=%fused_computation.40 | convolution fusion | flops 537001984 | bytes 4980736 | tf_op jit(solution)/shard_map/dot_general | solution.py:165
  238.6 73.0 %all-to-all-start.3 = ((bf16[32,32,128]{2,1,0:T(8,128)(2,1)}), bf16[32,32,128]{2,1,0:T(8,128)(2,1)S(1)}, u32[]{:S(2)}, u32[]{:S(2)}) async-start(bf16[32,32,128]{2,1,0:T(8,128)(2,1)} %bitcast.39), calls=%async_computation.3 | async-start | bytes 524288 | tf_op jit(solution)/shard_map/all_to_all | solution.py:167
  311.8 1.0 convolution_convert_fusion.1
  312.8 21.1 %all-to-all-done.3 = bf16[32,32,128]{2,1,0:T(8,128)(2,1)S(1)} async-done(((bf16[32,32,128]{2,1,0:T(8,128)(2,1)}), bf16[32,32,128]{2,1,0:T(8,128)(2,1)S(1)}, u32[]{:S(2)}, u32[]{:S(2)}) %all-to-all-start.3) | async-done | bytes 262176 | tf_op jit(solution)/shard_map/all_to_all | solution.py:167
  333.9 1.3 gather_fusion.1
  335.2 0.9 fusion.37
  (51 shorter events, 1.2 us)
Async XLA Ops:
  7.2 132.3 %copy-start = (bf16[1,2048,128]{2,1,0:T(8,128)(2,1)S(1)}, bf16[1,2048,128]{2,1,0:T(8,128)(2,1)}, u32[]{:S(2)}) copy-start(bf16[1,2048,128]{2,1,0:T(8,128)(2,1)} %param.27) | copy-start | bytes 1572868
  15.7 25.0 %copy-start.1 = (bf16[256,2048]{1,0:T(8,128)(2,1)S(1)}, bf16[256,2048]{1,0:T(8,128)(2,1)}, u32[]{:S(2)}) copy-start(bf16[256,2048]{1,0:T(8,128)(2,1)} %param.16) | copy-start | bytes 3145732
  23.9 39.0 %all-to-all-start.1 = ((bf16[32,2,2048]{2,1,0:T(2,128)(2,1)}), bf16[32,2,2048]{2,1,0:T(2,128)(2,1)S(1)}, u32[]{:S(2)}, u32[]{:S(2)}) async-start(bf16[32,2,2048]{2,1,0:T(2,128)(2,1)} %constant_dynamic-slice_fusion.1), calls=%async_computation.1 | async-start | bytes 524288 | tf_op jit(solution)/shard_map/all_to_all | solution.py:141
  65.5 7.0 %copy-start.5 = (bf16[2048,64]{0,1:T(8,128)(2,1)S(1)}, bf16[2048,64]{0,1:T(8,128)(2,1)}, u32[]{:S(2)}) copy-start(bf16[2048,64]{0,1:T(8,128)(2,1)} %param.19) | copy-start | bytes 786436
  65.5 7.0 %copy-start.8 = (f32[2048]{0:T(1024)S(1)}, f32[2048]{0:T(1024)}, u32[]{:S(2)}) copy-start(f32[2048]{0:T(1024)} %param.17) | copy-start | bytes 24580
  65.5 69.4 %all-to-all-start.2 = ((bf16[32,32,2048]{2,0,1:T(8,128)(2,1)}), bf16[32,32,2048]{2,0,1:T(8,128)(2,1)}, u32[]{:S(2)}, u32[]{:S(2)}) async-start(bf16[32,32,2048]{2,0,1:T(8,128)(2,1)} %bitcast.132), calls=%async_computation.2 | async-start | bytes 8388608 | tf_op jit(solution)/shard_map/all_to_all | solution.py:143
  72.5 1.0 copy-start.6
  72.5 58.1 %all-gather.9.cloned.1.call-start = ((), (), s32[]{:S(2)}) async-start(), calls=%async_computation.6 | async-start | bytes 1114112 | tf_op jit(solution)/shard_map/all_gather | solution.py:22
  74.6 86.0 %all-gather.5.cloned.1.call-start = ((), (), s32[]{:S(2)}) async-start(), calls=%async_computation.4 | async-start | bytes 3145728 | tf_op jit(solution)/shard_map/all_gather | solution.py:22
  133.1 101.2 %all-gather.7.cloned.1.call-start = ((), (), s32[]{:S(2)}) async-start(), calls=%async_computation.5 | async-start | bytes 4456448 | tf_op jit(solution)/shard_map/all_gather | solution.py:162
  139.5 1.3 copy-start.4
  140.7 2.7 copy-start.7
  169.2 69.5 %all-to-all-start = ((bf16[16,256,64]{1,2,0:T(8,128)(2,1)}), bf16[16,256,64]{1,2,0:T(8,128)(2,1)S(1)}, u32[]{:S(2)}, u32[]{:S(2)}) async-start(bf16[16,256,64]{1,2,0:T(8,128)(2,1)} %broadcast_in_dim.17), calls=%async_computation | async-start | bytes 1048576 | tf_op jit(solution)/shard_map/all_to_all | solution.py:35
  234.3 77.3 %copy-start.3 = (f32[128,4]{0,1:T(4,128)S(1)}, f32[128,4]{0,1:T(4,128)}, u32[]{:S(2)}) copy-start(f32[128,4]{0,1:T(4,128)} %param.26) | copy-start | bytes 6148
  234.3 77.5 %copy-start.2 = (bf16[1024,128]{1,0:T(8,128)(2,1)S(1)}, bf16[1024,128]{1,0:T(8,128)(2,1)}, u32[]{:S(2)}) copy-start(bf16[1024,128]{1,0:T(8,128)(2,1)} %param.22) | copy-start | bytes 786436
  238.6 95.3 %all-to-all-start.3 = ((bf16[32,32,128]{2,1,0:T(8,128)(2,1)}), bf16[32,32,128]{2,1,0:T(8,128)(2,1)S(1)}, u32[]{:S(2)}, u32[]{:S(2)}) async-start(bf16[32,32,128]{2,1,0:T(8,128)(2,1)} %bitcast.39), calls=%async_computation.3 | async-start | bytes 524288 | tf_op jit(solution)/shard_map/all_to_all | solution.py:167
Sparse Core Ops, SparseCore 0:
  75.9 54.6 all-gather.8
  133.2 27.3 all-gather.4
  163.6 70.6 all-gather.6
